TPU v7x, 32 devices: a whole 2x2x4 slice. The times are simulated.
32 devices in a mesh: ep: 8 (over z, core), tp: 4 (over y, x).
Axes of the slice: x: 2, y: 2, z: 4, core: 2. Of those that a mesh axis runs over, the one named last changes fastest.
Arguments:
- value_in: bfloat16 [8192, 1536], P('ep', 'tp'), may hold values from -6 to 6
- gate_in: bfloat16 [8192, 1536], P('ep', 'tp'), may hold values from -9 to 9
- conv_kernel: float32 [31, 1536], P(None, 'tp'), may hold values from -40 to 40
- norm_gain: float32 [1536], replicated, may hold values from 0.1 to 1.9
- norm_shift: float32 [1536], replicated, may hold values from -3 to 3
- out_weight: bfloat16 [1536, 2048], P(None, 'tp'), may hold values from -0.15625 to 0.15625
- expert_input: bfloat16 [1536, 2048], P('ep'), may hold values from -6 to 6
- expert_gain: float32 [2048], replicated, may hold values from 0.1 to 1.9
- route_ids: int32 [1536, 4], P('ep'), may hold values from 0 to 7, all different within a row; in each aligned block of 192 rows (0 to 191, 192 to 383, ...) at most 120 rows name the same one
- route_weights: float32 [1536, 4], P('ep'), may hold values from 0.2 to 1
- gate_weight: bfloat16 [8, 2048, 2048], P('ep', None, 'tp'), may hold values from -0.375 to 0.375
- up_weight: bfloat16 [8, 2048, 2048], P('ep', None, 'tp'), may hold values from -0.375 to 0.375
- down_weight: bfloat16 [8, 2048, 2048], P('ep', None, 'tp'), may hold values from -0.01953125 to 0.01953125
Outputs:
- mixed_out: bfloat16 [8192, 2048], P('ep', 'tp')
- routed_out: bfloat16 [1536, 2048], P('ep', 'tp')
Inputs may be any that keep to these rules, and one draw needn't show every extreme that they name: `route_ids`: each row names 4 different experts; among the rows of one index of ep (aligned blocks of 192 rows) no expert is named by more than 120 rows, and in some block one expert is named by exactly 120.
All inputs are finite; a program needn't handle non-finite values.
Results may differ from a plain program's by a relative error of at most 0.0071.
Values may be sent and summed in bfloat16 or wider, within the bound.
A program may use at most 64 MiB of HBM per device.

v0:
```python
import jax
import jax.numpy as jnp
from jax import lax
from jax.sharding import PartitionSpec as P


def shifted(block, axis, distance):
    devices = range(lax.axis_size(axis))
    route = [(i - distance, i) for i in devices if i - distance in devices]
    return lax.ppermute(block, axis, route)


def expert_tail(gate_pre, up_pre, down_weight):
    clamped = jnp.minimum(gate_pre, 7.0)
    upward = jnp.clip(up_pre, -7.0, 7.0)
    activation = ((upward + 1.0) * clamped * jax.nn.sigmoid(1.702 * clamped)).astype(jnp.bfloat16)
    weights = down_weight[0]
    summed = jnp.dot(
        lax.all_gather(activation, "tp", axis=1, tiled=True),
        weights,
        preferred_element_type=jnp.float32,
    )
    return summed.astype(jnp.bfloat16)


def finish(gate_pre, up_pre, down_weight, arrived_shape):
    outcome = expert_tail(gate_pre, up_pre, down_weight)
    outcome = outcome.reshape(arrived_shape[0], arrived_shape[1], outcome.shape[1])
    return lax.all_to_all(outcome, "ep", split_axis=0, concat_axis=0, tiled=True)


def body(
    value_in,
    gate_in,
    conv_kernel,
    norm_gain,
    norm_shift,
    out_weight,
    expert_input,
    expert_gain,
    route_ids,
    route_weights,
    gate_weight,
    up_weight,
    down_weight,
):
    gated_values = (
        value_in.astype(jnp.float32) * jax.nn.sigmoid(gate_in.astype(jnp.float32))
    ).astype(jnp.bfloat16)
    kernel_width = conv_kernel.shape[0]
    length_dev = gated_values.shape[0]
    before = shifted(gated_values[length_dev - (kernel_width - 1) :], "ep", 1)
    extended = jnp.concatenate([before, gated_values], 0).astype(jnp.float32)
    running = jnp.zeros(gated_values.shape, jnp.float32)
    for tap_index in range(kernel_width):
        running = (
            running + conv_kernel[tap_index][None, :] * extended[tap_index : tap_index + length_dev]
        )
    convolved = running.astype(jnp.bfloat16)
    gathered = lax.all_gather(convolved, "tp", axis=1, tiled=True).astype(jnp.float32)
    row_mean = jnp.mean(gathered, axis=1, keepdims=True)
    row_var = jnp.mean(jnp.square(gathered - row_mean), axis=1, keepdims=True)
    normed = (gathered - row_mean) * lax.rsqrt(row_var + 1e-05) * norm_gain[None, :] + norm_shift[
        None, :
    ]
    hidden = jax.nn.silu(normed).astype(jnp.bfloat16)
    mixed_out = jnp.dot(hidden, out_weight, preferred_element_type=jnp.float32).astype(jnp.bfloat16)
    experts = lax.axis_size("ep")
    row_count, model_width = expert_input.shape
    top_count = route_ids.shape[1]
    capacity = (5 * row_count * top_count + 4 * experts - 1) // (4 * experts)
    input_float = expert_input.astype(jnp.float32)
    feature_mean = jnp.mean(input_float, axis=1, keepdims=True)
    feature_var = jnp.mean(jnp.square(input_float - feature_mean), axis=1, keepdims=True)
    normed_rows = (
        (input_float - feature_mean) * lax.rsqrt(feature_var + 1e-05) * expert_gain[None, :]
    ).astype(jnp.bfloat16)
    expert_ids = route_ids.reshape(-1)
    onehot = (expert_ids[:, None] == jnp.arange(experts, dtype=jnp.int32)[None, :]).astype(
        jnp.int32
    )
    earlier = jnp.cumsum(onehot, axis=0) - onehot
    position = jnp.sum(earlier * onehot, axis=1)
    destination = expert_ids * capacity + position
    token_index = jnp.arange(expert_ids.shape[0], dtype=jnp.int32) // top_count
    slot_token = (
        jnp.full((experts * capacity,), row_count, jnp.int32).at[destination].set(token_index)
    )
    padded = jnp.concatenate([normed_rows, jnp.zeros((1, model_width), jnp.bfloat16)], 0)
    outgoing = padded[slot_token].reshape(experts, capacity, model_width)
    column_width = model_width // lax.axis_size("tp")
    columns = lax.dynamic_slice_in_dim(
        outgoing, lax.axis_index("tp") * column_width, column_width, 2
    )
    arrived = lax.all_to_all(columns, "ep", split_axis=0, concat_axis=0, tiled=True)
    slot_total = arrived.shape[0] * arrived.shape[1]
    portion = lax.all_gather(arrived, "tp", axis=2, tiled=True)
    flattened = portion.reshape(slot_total, portion.shape[2])
    gate_part = gate_weight[0]
    up_part = up_weight[0]
    gate_pre = jnp.dot(flattened, gate_part, preferred_element_type=jnp.float32)
    up_pre = jnp.dot(flattened, up_part, preferred_element_type=jnp.float32)
    results_home = finish(gate_pre, up_pre, down_weight, arrived.shape)
    picked = results_home.reshape(-1, results_home.shape[2])[destination]
    picked = picked.reshape(row_count, top_count, -1).astype(jnp.float32)
    routed_out = jnp.sum(picked * route_weights[:, :, None], axis=1).astype(jnp.bfloat16)
    return (mixed_out, routed_out)


def solution(mesh):
    return jax.shard_map(
        body,
        mesh=mesh,
        in_specs=(
            P("ep", "tp"),
            P("ep", "tp"),
            P(None, "tp"),
            P(),
            P(),
            P(None, "tp"),
            P("ep", None),
            P(),
            P("ep", None),
            P("ep", None),
            P("ep", None, "tp"),
            P("ep", None, "tp"),
            P("ep", None, "tp"),
        ),
        out_specs=(P("ep", "tp"), P("ep", "tp")),
        check_vma=False,
    )
```

profile of v0, /device:TPU:0, one launch (start us, length us, event | category | flops | bytes accessed | tf_op | source)
XLA Modules:
  0.0 255.0 jit_solution(3363373219548088409)
XLA Ops:
  7.2 0.9 copy.19
  8.4 0.7 broadcast_multiply_fusion
  9.1 1.7 reduce-window.6
  10.9 0.1 copy.21
  11.1 0.2 reduce-window.9
  11.3 0.1 copy.18
  11.7 3.4 %scatter_custom_fusion = s32[960]{0:T(1024)S(1)} fusion(s32[768]{0:T(1024)S(1)} %fusion.69, s32[768]{0:T(1024)S(1)} %add_select_fusion, s32[]{:T(128)} %constant.28.clone.1), kind=kCustom, calls=%fused_computation.118 | custom fusion | bytes 3844 | tf_op jit(solution)/shard_map/scatter | solution.py:87
  15.1 1.3 convert_reduce_fusion.1
  16.4 0.4 fusion.23
  16.8 0.4 fusion.25
  17.3 5.9 %gather_fusion = bf16[960,2048]{1,0:T(8,128)(2,1)} fusion(bf16[193,2048]{1,0:T(8,128)(2,1)S(1)} %concatenate.7, s32[1024]{0:T(1024)S(1)} %pad_clamp_fusion.1), kind=kCustom, calls=%fused_computation | custom fusion | bytes 7868160 | tf_op jit(solution)/shard_map/gather | solution.py:90
  23.2 1.3 constant_dynamic-slice_fusion
  24.5 31.5 %all_to_all.10 = bf16[8,120,512]{2,1,0:T(8,128)(2,1)} all-to-all(bf16[8,120,512]{2,1,0:T(8,128)(2,1)S(1)} %constant_dynamic-slice_fusion), channel_id=1, replica_groups=mesh['ep'=8,'tp'=4] {'ep'}, dimensions={0} | all-to-all | bytes 1966080 | tf_op jit(solution)/shard_map/all_to_all | solution.py:95
  56.1 1.6 multiply_convert_fusion.1
  57.7 1.5 collective-permute-start
  59.4 0.6 collective-permute-done
  60.0 0.2 maximum_convert_fusion
  60.2 6.8 %fusion.27 = bf16[1024,384]{1,0:T(8,128)(2,1)} fusion(f32[1054,384]{1,0:T(8,128)S(1)} %maximum_convert_fusion, f32[384]{0:T(512)S(1)} %get-tuple-element.31, f32[384]{0:T(512)S(1)} %get-tuple-element.32, f32[384]{0:T(512)S(1)} %get-tuple-element.3, f32[384]{0:T(512)S(1)} %get-tuple-element.4, f32[384]{0:T(512)S(1)} %get-tuple-element.5, ...), kind=kLoop, calls=%fused_computation.33 | loop fusion | flops 24379392 | bytes 49592832 | tf_op jit(solution)/shard_map/convert_element_type | solution.py:59
  67.1 38.4 %all-gather.6.cloned.1.call-done = bf16[8,120,2048]{2,1,0:T(8,128)(2,1)} async-done(((bf16[8,120,512]{2,1,0:T(8,128)(2,1)}), bf16[8,120,2048]{2,1,0:T(8,128)(2,1)}) %all-gather.6.cloned.1.call-update) | async-done | bytes 3932176 | tf_op jit(solution)/shard_map/all_gather | solution.py:97
  105.4 4.5 %fusion.15 = f32[960,512]{1,0:T(8,128)S(1)} fusion(bf16[960,2048]{1,0:T(8,128)(2,1)} %bitcast.36, bf16[1,2048,512]{2,1,0:T(8,128)(2,1)S(1)} %copy-done), kind=kOutput, calls=%fused_computation.19 | convolution fusion | flops 2013265920 | bytes 7995392 | tf_op jit(solution)/shard_map/dot_general | solution.py:101
  109.9 3.6 %multiply_convert_fusion = bf16[960,512]{1,0:T(8,128)(2,1)} fusion(f32[960,512]{1,0:T(8,128)S(1)} %fusion.15, bf16[960,2048]{1,0:T(8,128)(2,1)S(1)} %bitcast.37, bf16[1,2048,512]{2,1,0:T(8,128)(2,1)S(1)} %copy-done.8), kind=kOutput, calls=%fused_computation.23 | convolution fusion | flops 2018181120 | bytes 8978432 | tf_op jit(solution)/shard_map/dot_general | solution.py:102
  113.7 37.3 %all-gather.4.cloned.1.call-done = bf16[1024,1536]{1,0:T(8,128)(2,1)} async-done(((bf16[1024,384]{1,0:T(8,128)(2,1)}), bf16[1024,1536]{1,0:T(8,128)(2,1)}) %all-gather.4.cloned.1.call-update) | async-done | bytes 3145744 | tf_op jit(solution)/shard_map/all_gather | solution.py:60
  151.0 2.4 convert_reduce_fusion
  153.4 50.3 %all-gather.8.cloned.1.call-done = bf16[960,2048]{1,0:T(8,128)(2,1)} async-done(((bf16[960,512]{1,0:T(8,128)(2,1)}), bf16[960,2048]{1,0:T(8,128)(2,1)}) %all-gather.8.cloned.1.call-update) | async-done | bytes 3932176 | tf_op jit(solution)/shard_map/all_gather | solution.py:19
  203.7 5.9 %fusion.60 = bf16[960,512]{1,0:T(8,128)(2,1)} fusion(bf16[960,2048]{1,0:T(8,128)(2,1)} %all-gather.8.cloned.1.call-done, bf16[1,2048,512]{2,1,0:T(8,128)(2,1)} %param.25), kind=kOutput, calls=%fused_computation.96 | convolution fusion | flops 2013757440 | bytes 7012352 | tf_op jit(solution)/shard_map/dot_general | solution.py:18
  209.6 4.6 %all-to-all-start.1 = ((bf16[8,120,512]{2,1,0:T(8,128)(2,1)}), bf16[8,120,512]{2,1,0:T(8,128)(2,1)S(1)}, u32[]{:S(2)}, u32[]{:S(2)}) async-start(bf16[8,120,512]{2,1,0:T(8,128)(2,1)} %bitcast.33), calls=%async_computation.1 | async-start | bytes 1966080 | tf_op jit(solution)/shard_map/all_to_all | solution.py:29
  214.3 3.0 %fusion.2 = f32[1024]{0:T(1024)S(1)} fusion(bf16[1024,1536]{1,0:T(8,128)(2,1)} %all-gather.4.cloned.1.call-done, f32[1024]{0:T(1024)S(1)} %broadcast_multiply_fusion.1), kind=kLoop, calls=%fused_computation.7 | loop fusion | flops 6290432 | bytes 3153920 | tf_op jit(solution)/shard_map/reduce_sum | solution.py:62
  217.3 5.2 %fusion.57 = bf16[1024,512]{1,0:T(8,128)(2,1)} fusion(bf16[1536,512]{1,0:T(8,128)(2,1)} %param.18, bf16[1024,1536]{1,0:T(8,128)(2,1)S(1)} %copy-done.1, f32[1536]{0:T(1024)S(1)} %copy-done.9, f32[1536]{0:T(1024)S(1)} %copy-done.10, f32[1024]{0:T(1024)S(1)} %add_rsqrt_fusion, f32[1024]{0:T(1024)S(1)} %broadcast_multiply_fusion.1), kind=kOutput, calls=%fused_computation.95 | convolution fusion | flops 1626865664 | bytes 5787648 | tf_op jit(solution)/shard_map/dot_general | solution.py:67
  222.5 16.9 %all-to-all-done.1 = bf16[8,120,512]{2,1,0:T(8,128)(2,1)S(1)} async-done(((bf16[8,120,512]{2,1,0:T(8,128)(2,1)}), bf16[8,120,512]{2,1,0:T(8,128)(2,1)S(1)}, u32[]{:S(2)}, u32[]{:S(2)}) %all-to-all-start.1) | async-done | bytes 983072 | tf_op jit(solution)/shard_map/all_to_all | solution.py:29
  239.4 3.3 %gather_fusion.1 = bf16[768,512]{1,0:T(8,128)(2,1)} fusion(bf16[960,512]{1,0:T(8,128)(2,1)S(1)} %bitcast.31, s32[1024]{0:T(1024)S(1)} %pad_clamp_fusion), kind=kCustom, calls=%fused_computation.1 | custom fusion | bytes 1575936 | tf_op jit(solution)/shard_map/gather | solution.py:104
  242.7 2.6 %reshape.98 = f32[192,4,512]{2,1,0:T(4,128)} reshape(bf16[768,512]{1,0:T(8,128)(2,1)} %gather_fusion.1) | data formatting | bytes 2359296 | tf_op jit(solution)/shard_map/convert_element_type | solution.py:105
  245.3 3.1 %multiply_reduce_fusion = bf16[192,512]{1,0:T(8,128)(2,1)} fusion(f32[192,4,512]{2,1,0:T(4,128)} %reshape.98, f32[192,4]{1,0:T(8,128)S(1)} %copy.23), kind=kLoop, calls=%fused_computation.93 | loop fusion | flops 688128 | bytes 1772544 | tf_op jit(solution)/shard_map/reduce_sum | solution.py:106
  (49 shorter events, 1.3 us)
Async XLA Ops:
  7.2 98.3 %copy-start = (bf16[1,2048,512]{2,1,0:T(8,128)(2,1)S(1)}, bf16[1,2048,512]{2,1,0:T(8,128)(2,1)}, u32[]{:S(2)}) copy-start(bf16[1,2048,512]{2,1,0:T(8,128)(2,1)} %param.23) | copy-start | bytes 6291460
  7.2 9.2 %copy-start.2 = (bf16[192,2048]{1,0:T(8,128)(2,1)S(1)}, bf16[192,2048]{1,0:T(8,128)(2,1)}, u32[]{:S(2)}) copy-start(bf16[192,2048]{1,0:T(8,128)(2,1)} %param.19) | copy-start | bytes 2359300
  7.2 9.6 %copy-start.5 = (f32[2048]{0:T(1024)S(1)}, f32[2048]{0:T(1024)}, u32[]{:S(2)}) copy-start(f32[2048]{0:T(1024)} %param.20) | copy-start | bytes 24580
  7.2 98.2 %all-gather.6.cloned.1.call-start = ((), (), s32[]{:S(2)}) async-start(), calls=%async_computation.3 | async-start | bytes 4915200 | tf_op jit(solution)/shard_map/all_gather | solution.py:97
  24.5 31.6 %copy-start.3 = (bf16[1024,384]{1,0:T(8,128)(2,1)S(1)}, bf16[1024,384]{1,0:T(8,128)(2,1)}, u32[]{:S(2)}) copy-start(bf16[1024,384]{1,0:T(8,128)(2,1)} %param.14) | copy-start | bytes 2359300
  56.0 3.2 %copy-start.4 = (f32[31,384]{1,0:T(8,128)S(1)}, f32[31,384]{1,0:T(8,128)}, u32[]{:S(2)}) copy-start(f32[31,384]{1,0:T(8,128)} %param.15) | copy-start | bytes 142852
  56.1 94.9 %all-gather.4.cloned.1.call-start = ((), (), s32[]{:S(2)}) async-start(), calls=%async_computation.2 | async-start | bytes 3932160 | tf_op jit(solution)/shard_map/all_gather | solution.py:60
  57.7 2.3 collective-permute-start
  67.0 136.7 %all-gather.8.cloned.1.call-start = ((), (), s32[]{:S(2)}) async-start(), calls=%async_computation.4 | async-start | bytes 4915200 | tf_op jit(solution)/shard_map/all_gather | solution.py:19
  105.4 4.5 %copy-start.7 = (bf16[8,120,2048]{2,1,0:T(8,128)(2,1)S(1)}, bf16[8,120,2048]{2,1,0:T(8,128)(2,1)}, u32[]{:S(2)}) copy-start(bf16[8,120,2048]{2,1,0:T(8,128)(2,1)} %all-gather.6.cloned.1.call-done) | copy-start | bytes 11796484
  105.4 4.5 %copy-start.8 = (bf16[1,2048,512]{2,1,0:T(8,128)(2,1)S(1)}, bf16[1,2048,512]{2,1,0:T(8,128)(2,1)}, u32[]{:S(2)}) copy-start(bf16[1,2048,512]{2,1,0:T(8,128)(2,1)} %param.24) | copy-start | bytes 6291460
  109.9 3.6 %copy-start.6 = (f32[192,4]{0,1:T(4,128)S(1)}, f32[192,4]{0,1:T(4,128)}, u32[]{:S(2)}) copy-start(f32[192,4]{0,1:T(4,128)} %param.22) | copy-start | bytes 9220
  209.6 29.8 %all-to-all-start.1 = ((bf16[8,120,512]{2,1,0:T(8,128)(2,1)}), bf16[8,120,512]{2,1,0:T(8,128)(2,1)S(1)}, u32[]{:S(2)}, u32[]{:S(2)}) async-start(bf16[8,120,512]{2,1,0:T(8,128)(2,1)} %bitcast.33), calls=%async_computation.1 | async-start | bytes 1966080 | tf_op jit(solution)/shard_map/all_to_all | solution.py:29
  214.2 3.0 %copy-start.1 = (bf16[1024,1536]{1,0:T(8,128)(2,1)S(1)}, bf16[1024,1536]{1,0:T(8,128)(2,1)}, u32[]{:S(2)}) copy-start(bf16[1024,1536]{1,0:T(8,128)(2,1)} %all-gather.4.cloned.1.call-done) | copy-start | bytes 9437188
  214.2 3.0 %copy-start.9 = (f32[1536]{0:T(1024)S(1)}, f32[1536]{0:T(1024)}, u32[]{:S(2)}) copy-start(f32[1536]{0:T(1024)} %param.17) | copy-start | bytes 18436
  214.2 3.0 %copy-start.10 = (f32[1536]{0:T(1024)S(1)}, f32[1536]{0:T(1024)}, u32[]{:S(2)}) copy-start(f32[1536]{0:T(1024)} %param.16) | copy-start | bytes 18436
Sparse Core Ops, SparseCore 0:
  56.2 49.1 all-gather.5
  107.2 43.6 all-gather.3
  153.4 50.2 all-gather.7
where the time goes:
time: 255 us
  waiting for transfers between devices  144 us (56%)
  blocking collectives  31.5 us (12%)
  other arithmetic  21.9 us (9%)
  matrix products  19.1 us (7%)
  local copies, waits for them, and re-layouts  18.6 us (7%)
  between operations  14 us (5%)
  starting transfers between devices  6.19 us (2%)
    all_gather x1, waiting for transfers between devices, expert_tail(): lax.all_gather(activation, 'tp', axis=1, tiled=True)  50.3 us
    all_gather x1, waiting for transfers between devices, body(): portion = lax.all_gather(arrived, 'tp', axis=2, tiled=True)  38.4 us
    all_gather x1, waiting for transfers between devices, body(): lax.all_gather(convolved, 'tp', axis=1, tiled=True).astype(jnp.float32)  37.3 us
    all_to_all x1, blocking collectives, body(): lax.all_to_all(columns, 'ep', split_axis=0, concat_axis=0, tiled=True)  31.5 us
    all_to_all x1, waiting for transfers between devices, finish(): lax.all_to_all(outcome, 'ep', split_axis=0, concat_axis=0, tiled=True)  16.9 us
    convert_element_type x1, other arithmetic, body(): convolved = running.astype(jnp.bfloat16)  6.79 us
    dot_general x1, matrix products, expert_tail(): jnp.dot(lax.all_gather(activation, 'tp', axis=1, tiled=True), weights, pr...  5.93 us
    gather x1, local copies, waits for them, and re-layouts, body(): outgoing = padded[slot_token].reshape(experts, capacity, model_width)  5.91 us
  transfers between devices with their start and end apart: 5, of which 5 were waited for; matrix products, arithmetic and copies ran while one was open for 11% of the time, Pallas kernels for 0%

commit v1 on v0

--- a/solution.py
+++ b/solution.py
@@ -94,7 +94,7 @@
     )
     arrived = lax.all_to_all(columns, "ep", split_axis=0, concat_axis=0, tiled=True)
     slot_total = arrived.shape[0] * arrived.shape[1]
-    portion = lax.all_gather(arrived, "tp", axis=2, tiled=True)
+    portion = jnp.concatenate(jax.lax.all_gather(arrived, "tp"), axis=2)
     flattened = portion.reshape(slot_total, portion.shape[2])
     gate_part = gate_weight[0]
     up_part = up_weight[0]

time: 255 us -> 256 us (level)
  local copies, waits for them, and re-layouts: 18.6 us -> 25.1 us
  waiting for transfers between devices: 144 us -> 139 us
    reshape x0 -> x1, local copies, waits for them, and re-layouts: none -> 5.15 us  [body(): portion = jnp.concatenate(jax.lax.all_gather(arrived, 'tp'), axis=2)]
    all_gather x1, waiting for transfers between devices: 37.3 us -> 33.1 us  [body(): lax.all_gather(convolved, 'tp', axis=1, tiled=True).astype(jnp.float32)]
  transfers between devices with their start and end apart: 5 -> 5, of which waited for: 5 -> 5; matrix products, arithmetic and copies ran while one was open for 11% -> 12% of each run, Pallas kernels for 0% -> 0%
where the time goes in v1:
time: 256 us; the launch traced here: 255 us
  waiting for transfers between devices  139 us (54%)
  blocking collectives  31.5 us (12%)
  local copies, waits for them, and re-layouts  25.1 us (10%)
  other arithmetic  21.9 us (9%)
  matrix products  16.8 us (7%)
  between operations  14 us (5%)
  starting transfers between devices  6.38 us (2%)
    all_gather x1, waiting for transfers between devices, expert_tail(): lax.all_gather(activation, 'tp', axis=1, tiled=True)  50.3 us
    all_gather x1, waiting for transfers between devices, body(): portion = jnp.concatenate(jax.lax.all_gather(arrived, 'tp'), axis=2)  38.3 us
    all_gather x1, waiting for transfers between devices, body(): lax.all_gather(convolved, 'tp', axis=1, tiled=True).astype(jnp.float32)  33.1 us
    all_to_all x1, blocking collectives, body(): lax.all_to_all(columns, 'ep', split_axis=0, concat_axis=0, tiled=True)  31.5 us
    all_to_all x1, waiting for transfers between devices, finish(): lax.all_to_all(outcome, 'ep', split_axis=0, concat_axis=0, tiled=True)  16.9 us
    convert_element_type x1, other arithmetic, body(): convolved = running.astype(jnp.bfloat16)  6.79 us
    dot_general x1, matrix products, expert_tail(): jnp.dot(lax.all_gather(activation, 'tp', axis=1, tiled=True), weights, pr...  5.93 us
    gather x1, local copies, waits for them, and re-layouts, body(): outgoing = padded[slot_token].reshape(experts, capacity, model_width)  5.91 us
  transfers between devices with their start and end apart: 5, of which 5 were waited for; matrix products, arithmetic and copies ran while one was open for 12% of the time, Pallas kernels for 0%

profile of v1, /device:TPU:0, one launch (start us, length us, event | category | flops | bytes accessed | tf_op | source)
XLA Modules:
  0.0 255.1 jit_solution(5988340318084474093)
XLA Ops:
  7.2 0.9 copy.32
  8.4 0.7 broadcast_multiply_fusion
  9.1 1.7 reduce-window.6
  11.7 3.4 %scatter_custom_fusion = s32[960]{0:T(1024)S(1)} fusion(s32[768]{0:T(1024)S(1)} %fusion.69, s32[768]{0:T(1024)S(1)} %add_select_fusion, s32[]{:T(128)} %constant.28.clone.1), kind=kCustom, calls=%fused_computation.118 | custom fusion | bytes 3844 | tf_op jit(solution)/shard_map/scatter | solution.py:87
  15.1 1.3 convert_reduce_fusion.1
  16.4 0.4 fusion.23
  16.8 0.4 fusion.25
  17.3 5.9 %gather_fusion = bf16[960,2048]{1,0:T(8,128)(2,1)} fusion(bf16[193,2048]{1,0:T(8,128)(2,1)S(1)} %concatenate.7, s32[1024]{0:T(1024)S(1)} %pad_clamp_fusion.1), kind=kCustom, calls=%fused_computation | custom fusion | bytes 7868160 | tf_op jit(solution)/shard_map/gather | solution.py:90
  23.2 1.3 constant_dynamic-slice_fusion
  24.5 31.5 %all_to_all.10 = bf16[8,120,512]{2,1,0:T(8,128)(2,1)} all-to-all(bf16[8,120,512]{2,1,0:T(8,128)(2,1)S(1)} %constant_dynamic-slice_fusion), channel_id=1, replica_groups=mesh['ep'=8,'tp'=4] {'ep'}, dimensions={0} | all-to-all | bytes 1966080 | tf_op jit(solution)/shard_map/all_to_all | solution.py:95
  56.1 1.6 multiply_convert_fusion.1
  57.7 1.5 collective-permute-start
  59.4 0.6 collective-permute-done
  60.0 0.2 maximum_convert_fusion
  60.2 6.8 %fusion.27 = bf16[1024,384]{1,0:T(8,128)(2,1)} fusion(f32[1054,384]{1,0:T(8,128)S(1)} %maximum_convert_fusion, f32[384]{0:T(512)S(1)} %get-tuple-element.31, f32[384]{0:T(512)S(1)} %get-tuple-element.32, f32[384]{0:T(512)S(1)} %get-tuple-element.3, f32[384]{0:T(512)S(1)} %get-tuple-element.4, f32[384]{0:T(512)S(1)} %get-tuple-element.5, ...), kind=kLoop, calls=%fused_computation.33 | loop fusion | flops 24379392 | bytes 49592832 | tf_op jit(solution)/shard_map/convert_element_type | solution.py:59
  67.0 0.2 all-gather.7.cloned.1.call-start
  67.2 38.3 %all-gather.9.cloned.1.call-done = bf16[32,120,512]{2,1,0:T(8,128)(2,1)} async-done(((bf16[8,120,512]{2,1,0:T(8,128)(2,1)}), bf16[32,120,512]{2,1,0:T(8,128)(2,1)}) %all-gather.9.cloned.1.call-update) | async-done | bytes 3932176 | tf_op jit(solution)/shard_map/all_gather | solution.py:97
  105.6 5.1 %copy.36 = bf16[8,120,4,512]{3,2,1,0:T(4,128)(2,1)S(1)} copy(bf16[8,120,4,512]{3,1,0,2:T(8,128)(2,1)} %bitcast.39) | data formatting | bytes 7864320 | tf_op jit(solution)/shard_map/reshape | solution.py:97
  110.7 1.3 copy.38
  112.0 2.2 fusion.15
  114.2 3.6 %multiply_convert_fusion = bf16[960,512]{1,0:T(8,128)(2,1)} fusion(f32[960,512]{1,0:T(8,128)S(1)} %fusion.15, bf16[960,2048]{1,0:T(8,128)(2,1)S(1)} %bitcast.41, bf16[1,2048,512]{2,1,0:T(8,128)(2,1)S(1)} %copy-done.7), kind=kOutput, calls=%fused_computation.23 | convolution fusion | flops 2018181120 | bytes 8978432 | tf_op jit(solution)/shard_map/dot_general | solution.py:102
  118.0 33.1 %all-gather.5.cloned.1.call-done = bf16[1024,1536]{1,0:T(8,128)(2,1)} async-done(((bf16[1024,384]{1,0:T(8,128)(2,1)}), bf16[1024,1536]{1,0:T(8,128)(2,1)}) %all-gather.5.cloned.1.call-update) | async-done | bytes 3145744 | tf_op jit(solution)/shard_map/all_gather | solution.py:60
  151.1 2.4 convert_reduce_fusion
  153.5 50.3 %all-gather.7.cloned.1.call-done = bf16[960,2048]{1,0:T(8,128)(2,1)} async-done(((bf16[960,512]{1,0:T(8,128)(2,1)}), bf16[960,2048]{1,0:T(8,128)(2,1)}) %all-gather.7.cloned.1.call-update) | async-done | bytes 3932176 | tf_op jit(solution)/shard_map/all_gather | solution.py:19
  203.8 5.9 %fusion.60 = bf16[960,512]{1,0:T(8,128)(2,1)} fusion(bf16[960,2048]{1,0:T(8,128)(2,1)} %all-gather.7.cloned.1.call-done, bf16[1,2048,512]{2,1,0:T(8,128)(2,1)} %param.25), kind=kOutput, calls=%fused_computation.96 | convolution fusion | flops 2013757440 | bytes 7012352 | tf_op jit(solution)/shard_map/dot_general | solution.py:18
  209.7 4.6 %all-to-all-start.1 = ((bf16[8,120,512]{2,1,0:T(8,128)(2,1)}), bf16[8,120,512]{2,1,0:T(8,128)(2,1)S(1)}, u32[]{:S(2)}, u32[]{:S(2)}) async-start(bf16[8,120,512]{2,1,0:T(8,128)(2,1)} %bitcast.42), calls=%async_computation.1 | async-start | bytes 1966080 | tf_op jit(solution)/shard_map/all_to_all | solution.py:29
  214.4 3.0 %fusion.2 = f32[1024]{0:T(1024)S(1)} fusion(bf16[1024,1536]{1,0:T(8,128)(2,1)} %all-gather.5.cloned.1.call-done, f32[1024]{0:T(1024)S(1)} %broadcast_multiply_fusion.1), kind=kLoop, calls=%fused_computation.7 | loop fusion | flops 6290432 | bytes 3153920 | tf_op jit(solution)/shard_map/reduce_sum | solution.py:62
  217.4 5.2 %fusion.57 = bf16[1024,512]{1,0:T(8,128)(2,1)} fusion(bf16[1536,512]{1,0:T(8,128)(2,1)} %param.18, bf16[1024,1536]{1,0:T(8,128)(2,1)S(1)} %copy-done.1, f32[1536]{0:T(1024)S(1)} %copy-done.8, f32[1536]{0:T(1024)S(1)} %copy-done.9, f32[1024]{0:T(1024)S(1)} %add_rsqrt_fusion, f32[1024]{0:T(1024)S(1)} %broadcast_multiply_fusion.1), kind=kOutput, calls=%fused_computation.95 | convolution fusion | flops 1626865664 | bytes 5787648 | tf_op jit(solution)/shard_map/dot_general | solution.py:67
  222.6 16.9 %all-to-all-done.1 = bf16[8,120,512]{2,1,0:T(8,128)(2,1)S(1)} async-done(((bf16[8,120,512]{2,1,0:T(8,128)(2,1)}), bf16[8,120,512]{2,1,0:T(8,128)(2,1)S(1)}, u32[]{:S(2)}, u32[]{:S(2)}) %all-to-all-start.1) | async-done | bytes 983072 | tf_op jit(solution)/shard_map/all_to_all | solution.py:29
  239.5 3.3 %gather_fusion.1 = bf16[768,512]{1,0:T(8,128)(2,1)} fusion(bf16[960,512]{1,0:T(8,128)(2,1)S(1)} %bitcast.36, s32[1024]{0:T(1024)S(1)} %pad_clamp_fusion), kind=kCustom, calls=%fused_computation.1 | custom fusion | bytes 1575936 | tf_op jit(solution)/shard_map/gather | solution.py:104
  242.9 2.6 %reshape.98 = f32[192,4,512]{2,1,0:T(4,128)} reshape(bf16[768,512]{1,0:T(8,128)(2,1)} %gather_fusion.1) | data formatting | bytes 2359296 | tf_op jit(solution)/shard_map/convert_element_type | solution.py:105
  245.4 3.1 %multiply_reduce_fusion = bf16[192,512]{1,0:T(8,128)(2,1)} fusion(f32[192,4,512]{2,1,0:T(4,128)} %reshape.98, f32[192,4]{1,0:T(8,128)S(1)} %copy.37), kind=kLoop, calls=%fused_computation.93 | loop fusion | flops 688128 | bytes 1772544 | tf_op jit(solution)/shard_map/reduce_sum | solution.py:106
  (49 shorter events, 1.6 us)
Async XLA Ops:
  7.2 104.9 %copy-start = (bf16[1,2048,512]{2,1,0:T(8,128)(2,1)S(1)}, bf16[1,2048,512]{2,1,0:T(8,128)(2,1)}, u32[]{:S(2)}) copy-start(bf16[1,2048,512]{2,1,0:T(8,128)(2,1)} %param.23) | copy-start | bytes 6291460
  7.2 9.2 %copy-start.2 = (bf16[192,2048]{1,0:T(8,128)(2,1)S(1)}, bf16[192,2048]{1,0:T(8,128)(2,1)}, u32[]{:S(2)}) copy-start(bf16[192,2048]{1,0:T(8,128)(2,1)} %param.19) | copy-start | bytes 2359300
  7.2 9.6 %copy-start.5 = (f32[2048]{0:T(1024)S(1)}, f32[2048]{0:T(1024)}, u32[]{:S(2)}) copy-start(f32[2048]{0:T(1024)} %param.20) | copy-start | bytes 24580
  7.2 98.4 %all-gather.9.cloned.1.call-start = ((), (), s32[]{:S(2)}) async-start(), calls=%async_computation.4 | async-start | bytes 4915200 | tf_op jit(solution)/shard_map/all_gather | solution.py:97
  24.5 31.6 %copy-start.3 = (bf16[1024,384]{1,0:T(8,128)(2,1)S(1)}, bf16[1024,384]{1,0:T(8,128)(2,1)}, u32[]{:S(2)}) copy-start(bf16[1024,384]{1,0:T(8,128)(2,1)} %param.14) | copy-start | bytes 2359300
  56.0 3.2 %copy-start.4 = (f32[31,384]{1,0:T(8,128)S(1)}, f32[31,384]{1,0:T(8,128)}, u32[]{:S(2)}) copy-start(f32[31,384]{1,0:T(8,128)} %param.15) | copy-start | bytes 142852
  56.1 95.0 %all-gather.5.cloned.1.call-start = ((), (), s32[]{:S(2)}) async-start(), calls=%async_computation.2 | async-start | bytes 3932160 | tf_op jit(solution)/shard_map/all_gather | solution.py:60
  57.7 2.3 collective-permute-start
  67.0 136.8 %all-gather.7.cloned.1.call-start = ((), (), s32[]{:S(2)}) async-start(), calls=%async_computation.3 | async-start | bytes 4915200 | tf_op jit(solution)/shard_map/all_gather | solution.py:19
  112.0 2.2 copy-start.7
  114.2 3.6 %copy-start.6 = (f32[192,4]{0,1:T(4,128)S(1)}, f32[192,4]{0,1:T(4,128)}, u32[]{:S(2)}) copy-start(f32[192,4]{0,1:T(4,128)} %param.22) | copy-start | bytes 9220
  209.7 29.8 %all-to-all-start.1 = ((bf16[8,120,512]{2,1,0:T(8,128)(2,1)}), bf16[8,120,512]{2,1,0:T(8,128)(2,1)S(1)}, u32[]{:S(2)}, u32[]{:S(2)}) async-start(bf16[8,120,512]{2,1,0:T(8,128)(2,1)} %bitcast.42), calls=%async_computation.1 | async-start | bytes 1966080 | tf_op jit(solution)/shard_map/all_to_all | solution.py:29
  214.4 3.0 %copy-start.1 = (bf16[1024,1536]{1,0:T(8,128)(2,1)S(1)}, bf16[1024,1536]{1,0:T(8,128)(2,1)}, u32[]{:S(2)}) copy-start(bf16[1024,1536]{1,0:T(8,128)(2,1)} %all-gather.5.cloned.1.call-done) | copy-start | bytes 9437188
  214.4 3.0 %copy-start.8 = (f32[1536]{0:T(1024)S(1)}, f32[1536]{0:T(1024)}, u32[]{:S(2)}) copy-start(f32[1536]{0:T(1024)} %param.17) | copy-start | bytes 18436
  214.4 3.0 %copy-start.9 = (f32[1536]{0:T(1024)S(1)}, f32[1536]{0:T(1024)}, u32[]{:S(2)}) copy-start(f32[1536]{0:T(1024)} %param.16) | copy-start | bytes 18436
Sparse Core Ops, SparseCore 0:
  56.2 49.3 all-gather.8
  107.4 43.6 all-gather.4
  153.5 50.2 all-gather.6
